TPU v7x, 32 devices: a whole 2x2x4 slice. The times are simulated.
32 devices in a mesh: sp: 8 (over z, x), tp: 4 (over y, core).
Axes of the slice: x: 2, y: 2, z: 4, core: 2. Of those that a mesh axis runs over, the one named last changes fastest.
Arguments:
- wide_query: bfloat16 [4096, 1536], P('sp', 'tp'), may hold values from -6 to 6
- wide_key: bfloat16 [4096, 1536], P('sp', 'tp'), may hold values from -6 to 6
- wide_value: bfloat16 [4096, 1536], P('sp', 'tp'), may hold values from -6 to 6
- wide_gate: bfloat16 [4096, 1536], P('sp', 'tp'), may hold values from -6 to 6
- narrow_query: bfloat16 [4096, 512], P('sp', 'tp'), may hold values from -6 to 6
- narrow_key: bfloat16 [4096, 512], P('sp', 'tp'), may hold values from -6 to 6
- narrow_value: bfloat16 [4096, 512], P('sp', 'tp'), may hold values from -6 to 6
- narrow_gate: bfloat16 [4096, 512], P('sp', 'tp'), may hold values from -6 to 6
- wide_decay: float32 [12, 4096], P('tp', 'sp'), may hold values from -1 to 0
- narrow_decay: float32 [8, 4096], P('tp', 'sp'), may hold values from -1 to 0
- residual: bfloat16 [4096, 2048], P(('sp', 'tp')), may hold values from -6 to 6
- wide_out: bfloat16 [1536, 2048], P('tp'), may hold values from -0.125 to 0.125
- narrow_out: bfloat16 [512, 2048], P('tp'), may hold values from -0.125 to 0.125
- up_weight: bfloat16 [2048, 8192], P('sp', 'tp'), may hold values from -0.125 to 0.125
- down_weight: bfloat16 [8192, 2048], P('tp', 'sp'), may hold values from -0.0625 to 0.0625
- gain_mix: float32 [2048], replicated, may hold values from 0.1 to 1.9
- gain_pre: float32 [2048], replicated, may hold values from 0.1 to 1.9
- gain_mlp: float32 [2048], replicated, may hold values from 0.1 to 1.9
Outputs:
- result: bfloat16 [4096, 2048], P(('sp', 'tp'))
All inputs are finite; a program needn't handle non-finite values.
Results may differ from a plain program's by a relative error of at most 0.02.
Values may be sent and summed in bfloat16 or wider, within the bound.
A program may use at most 128 MiB of HBM per device.

v0:
```python
import jax
import jax.numpy as jnp
from jax import lax
from jax.sharding import PartitionSpec as P

WIDE_DIM = 128
NARROW_DIM = 64
SPAN = 128
epsilon = 1e-06


def prefix_2(array, axis, join, neutral):
    place = lax.axis_index(axis)
    gathered = jax.tree.map(
        lambda a, kind: lax.all_gather(a.astype(kind), axis),
        array,
        (jnp.bfloat16, jnp.bfloat16, jnp.bfloat16, jnp.bfloat16),
    )
    state = jax.tree.map(lambda a, e: jnp.zeros_like(a) + jnp.asarray(e, a.dtype), array, neutral)

    def one(turn, state):
        return join(
            state,
            jax.tree.map(
                lambda a, own: lax.dynamic_index_in_dim(a, turn, 0, False).astype(own.dtype),
                gathered,
                array,
            ),
        )

    return lax.fori_loop(0, place, one, state)


def rotate(packed, head_dim, positions):
    length = packed.shape[0]
    grouped = packed.astype(jnp.float32).reshape(length, -1, head_dim)
    halfway = head_dim // 2
    inverse = 10000.0 ** (-jnp.arange(0, head_dim, 2, dtype=jnp.float32) / head_dim)
    angles = positions.astype(jnp.float32)[:, None] * inverse[None, :]
    cosine_table = jnp.cos(angles)[:, None, :]
    sine_table = jnp.sin(angles)[:, None, :]
    leading = grouped[..., :halfway]
    trailing = grouped[..., halfway:]
    return jnp.concatenate(
        [
            leading * cosine_table - trailing * sine_table,
            leading * sine_table + trailing * cosine_table,
        ],
        axis=-1,
    )


def rms_scale(values, gain_vector):
    return (
        values
        * lax.rsqrt(jnp.mean(values * values, axis=-1, keepdims=True) + epsilon)
        * gain_vector
    )


def span_terms(query, key, value, log_decay, head_dim, offset):
    length = query.shape[0]
    count_of_heads = query.shape[1] // head_dim
    span_count = length // SPAN
    shaped = (span_count, SPAN, count_of_heads, head_dim)
    positions = offset + jnp.arange(length, dtype=jnp.int32)
    queries = rotate(query, head_dim, positions).astype(jnp.bfloat16).reshape(shaped)
    keys_full = (rotate(key, head_dim, positions) * head_dim ** (-0.5)).reshape(shaped)
    keys_half = keys_full.astype(jnp.bfloat16)
    values_all = value.reshape(shaped)
    cumulative = jnp.cumsum(log_decay.T.reshape(span_count, SPAN, count_of_heads), axis=1)
    causal = jnp.arange(SPAN)[:, None] >= jnp.arange(SPAN)[None, :]
    scores = jnp.einsum("nihd,njhd->nhij", queries, keys_half, preferred_element_type=jnp.float32)
    decay_rows = cumulative.transpose(0, 2, 1)
    log_gaps = jnp.where(causal, decay_rows[..., :, None] - decay_rows[..., None, :], -jnp.inf)
    weights = (scores * jnp.exp(log_gaps)).astype(jnp.bfloat16)
    within = jnp.einsum("nhij,njhd->nihd", weights, values_all, preferred_element_type=jnp.float32)
    span_total = cumulative[:, -1, :]
    scaled = (keys_full * jnp.exp(span_total[:, None, :] - cumulative)[..., None]).astype(
        jnp.bfloat16
    )
    own_state = jnp.einsum(
        "njhd,njhe->nhde", scaled, values_all, preferred_element_type=jnp.float32
    )

    def advance(carried, inputs):
        decay_sum, contribution = inputs
        return (carried * jnp.exp(decay_sum)[:, None, None] + contribution, carried)

    initial = jnp.zeros((count_of_heads, head_dim, head_dim), jnp.float32)
    closing, before = lax.scan(advance, initial, (span_total, own_state))
    device_decay = jnp.exp(jnp.sum(span_total, axis=0))
    return (queries, cumulative, within, span_total, before, closing, device_decay)


def finish(parts, prefix, gate, head_dim):
    queries, cumulative, within, span_total, before, closing, device_decay = parts
    length = gate.shape[0]
    earlier = jnp.cumsum(span_total, axis=0) - span_total
    entering = (prefix[None] * jnp.exp(earlier)[:, :, None, None] + before).astype(jnp.bfloat16)
    across = (
        jnp.einsum("nihd,nhde->nihe", queries, entering, preferred_element_type=jnp.float32)
        * jnp.exp(cumulative)[..., None]
    )
    output = (within + across).reshape(length, -1, head_dim)
    normed = output * lax.rsqrt(jnp.mean(output * output, axis=-1, keepdims=True) + epsilon)
    return (normed.reshape(length, -1) * jax.nn.silu(gate.astype(jnp.float32))).astype(jnp.bfloat16)


def combine_states(former, latter):
    return (
        former[0] * latter[0],
        former[1] * latter[0][:, None, None] + latter[1],
        former[2] * latter[2],
        former[3] * latter[2][:, None, None] + latter[3],
    )


def local(
    wide_query,
    wide_key,
    wide_value,
    wide_gate,
    narrow_query,
    narrow_key,
    narrow_value,
    narrow_gate,
    wide_decay,
    narrow_decay,
    residual,
    wide_out,
    narrow_out,
    up_weight,
    down_weight,
    gain_mix,
    gain_pre,
    gain_mlp,
):
    length = wide_query.shape[0]
    offset = lax.axis_index("sp") * length
    wide_parts = span_terms(wide_query, wide_key, wide_value, wide_decay, WIDE_DIM, offset)
    narrow_parts = span_terms(
        narrow_query, narrow_key, narrow_value, narrow_decay, NARROW_DIM, offset
    )
    identity = (
        jnp.ones_like(wide_parts[6]),
        jnp.zeros_like(wide_parts[5]),
        jnp.ones_like(narrow_parts[6]),
        jnp.zeros_like(narrow_parts[5]),
    )
    prefixes = prefix_2(
        (wide_parts[6], wide_parts[5], narrow_parts[6], narrow_parts[5]),
        "sp",
        combine_states,
        identity,
    )
    wide_mixed = finish(wide_parts, prefixes[1], wide_gate, WIDE_DIM)
    narrow_mixed = finish(narrow_parts, prefixes[3], narrow_gate, NARROW_DIM)
    wide_rows, narrow_rows = (
        lax.all_to_all(wide_mixed, "tp", split_axis=0, concat_axis=1, tiled=True),
        lax.all_to_all(narrow_mixed, "tp", split_axis=0, concat_axis=1, tiled=True),
    )
    wide_whole, narrow_whole = (
        lax.all_gather(wide_out, "tp", axis=0, tiled=True),
        lax.all_gather(narrow_out, "tp", axis=0, tiled=True),
    )
    projected = jnp.dot(wide_rows, wide_whole, preferred_element_type=jnp.float32) + jnp.dot(
        narrow_rows, narrow_whole, preferred_element_type=jnp.float32
    )
    updated = (residual.astype(jnp.float32) + rms_scale(projected, gain_mix)).astype(jnp.bfloat16)
    normed = rms_scale(updated.astype(jnp.float32), gain_pre).astype(jnp.bfloat16)
    block_rows = lax.all_gather(normed, "tp", axis=0, tiled=True)
    rectified = jax.nn.relu(
        jnp.dot(
            block_rows,
            lax.all_gather(up_weight, "sp", axis=0, tiled=True),
            preferred_element_type=jnp.float32,
        )
    )
    hidden = (rectified * rectified).astype(jnp.bfloat16)
    partial_terms = jnp.dot(
        hidden,
        lax.all_gather(down_weight, "sp", axis=1, tiled=True),
        preferred_element_type=jnp.float32,
    )
    lowered = lax.psum_scatter(
        partial_terms.astype(jnp.bfloat16), "tp", scatter_dimension=0, tiled=True
    ).astype(jnp.float32)
    return (updated.astype(jnp.float32) + rms_scale(lowered, gain_mlp)).astype(jnp.bfloat16)


def solution(mesh):
    return jax.shard_map(
        local,
        mesh=mesh,
        in_specs=(
            P("sp", "tp"),
            P("sp", "tp"),
            P("sp", "tp"),
            P("sp", "tp"),
            P("sp", "tp"),
            P("sp", "tp"),
            P("sp", "tp"),
            P("sp", "tp"),
            P("tp", "sp"),
            P("tp", "sp"),
            P(("sp", "tp"), None),
            P("tp", None),
            P("tp", None),
            P("sp", "tp"),
            P("tp", "sp"),
            P(),
            P(),
            P(),
        ),
        out_specs=P(("sp", "tp"), None),
        check_vma=False,
    )
```

profile of v0, /device:TPU:0, one launch (start us, length us, event | category | flops | bytes accessed | tf_op | source)
XLA Modules:
  0.0 507.7 jit_solution(15633803309684791243)
XLA Ops:
  6.5 0.7 all-gather.10.cloned.1.call-update
  7.3 0.7 all-gather.12.cloned.1.call-update
  8.1 1.2 copy.77
  10.2 1.0 subtract_convert_fusion
  12.6 0.8 fusion.76
  13.6 0.8 fusion.33
  14.4 3.3 while.42
  14.4 0.7 bitcast_dynamic-update-slice_fusion.8
  15.2 0.7 bitcast_dynamic-update-slice_fusion.8
  16.0 0.7 bitcast_dynamic-update-slice_fusion.8
  16.9 0.7 bitcast_dynamic-update-slice_fusion.8
  17.7 33.8 %all-gather.1 = bf16[24,128,128]{2,1,0:T(8,128)(2,1)S(1)} all-gather(bf16[3,128,128]{2,1,0:T(8,128)(2,1)S(1)} %convert_element_type.154), channel_id=3, replica_groups=mesh['sp'=8,'tp'=4] {'sp'}, dimensions={0}, use_global_device_ids=true | all-gather | bytes 884736 | tf_op jit(solution)/shard_map/all_gather | solution.py:15
  51.6 1.0 multiply_cosine_fusion.1
  52.5 1.7 copy.93
  54.2 0.9 convert.30
  55.1 1.7 copy.106
  56.8 0.9 convert.31
  57.8 1.6 fusion.61
  59.4 0.7 bitcast_dynamic-update-slice_fusion.3
  60.1 0.9 copy.122
  61.0 1.2 reduce_window_sum.45
  62.2 0.6 fusion.75
  63.0 0.9 fusion.74
  63.9 1.1 copy.97
  65.0 1.8 reshape.384
  66.7 1.7 copy.99
  68.5 1.6 bitcast_dynamic-update-slice_fusion.2
  70.0 1.9 fusion.54
  71.9 6.2 %while.43 = (s32[]{:T(128)}, f32[2,64,64]{2,1,0:T(8,128)S(1)}, f32[4,2,64,64]{3,2,1,0:T(8,128)}, f32[4,2]{1,0:T(4,128)S(1)}, f32[4,2,64,64]{3,2,1,0:T(8,128)}, /*index=5*/s32[]{:T(128)}, s32[]{:T(128)}) while((s32[]{:T(128)}, f32[2,64,64]{2,1,0:T(8,128)S(1)}, f32[4,2,64,64]{3,2,1,0:T(8,128)}, f32[4,2]{1,0:T(4,128)S(1)}, ...), condition=%wide.region_7.8_spmd.clone, body=%wide.region_6.7_spmd.clone.sunk | while | flops 32771 | bytes 197240 | solution.py:91
  71.9 0.6 bitcast_dynamic-update-slice_fusion.9
  72.5 0.9 bitcast_add_fusion.5
  73.5 0.6 bitcast_dynamic-update-slice_fusion.9
  74.1 0.9 bitcast_add_fusion.5
  75.0 0.6 bitcast_dynamic-update-slice_fusion.9
  75.7 0.9 bitcast_add_fusion.5
  76.6 0.6 bitcast_dynamic-update-slice_fusion.9
  77.2 0.9 bitcast_add_fusion.5
  78.1 32.7 %all-gather.3 = bf16[16,64,64]{2,1,0:T(8,128)(2,1)} all-gather(bf16[2,64,64]{2,1,0:T(8,128)(2,1)S(1)} %convert_element_type.158), channel_id=5, replica_groups=mesh['sp'=8,'tp'=4] {'sp'}, dimensions={0}, use_global_device_ids=true | all-gather | bytes 147456 | tf_op jit(solution)/shard_map/all_gather | solution.py:15
  110.9 0.7 exponential_convert_fusion
  111.6 1.3 dynamic-slice
  114.6 21.4 %all-reduce.2 = (bf16[24]{0:T(256)(128)(2,1)S(1)}, bf16[16]{0:T(256)(128)(2,1)S(1)}) all-reduce(bf16[24]{0:T(256)(128)(2,1)S(1)} %dynamic-update-slice, bf16[16]{0:T(256)(128)(2,1)S(1)} %dynamic-update-slice.1), channel_id=2, replica_groups=mesh['sp'=8,'tp'=4] {'sp'}, use_global_device_ids=true, to_apply=%add | all-reduce | flops 40 | bytes 160
  136.2 1.0 concatenate.34
  137.5 1.7 concatenate.35
  139.1 1.2 copy.79
  140.3 1.1 copy.102
  142.1 2.6 fusion.8
  144.7 3.1 multiply_reduce_fusion.1
  147.8 1.7 copy.103
  149.6 1.2 copy.104
  151.0 0.8 copy_bitcast_fusion
  151.8 3.5 all-to-all-start
  157.2 0.7 copy_bitcast_fusion.1
  157.8 4.8 all-to-all-done
  162.7 3.3 all-to-all-start.1
  166.3 3.8 fusion.77
  170.6 2.1 multiply_reduce_fusion
  173.1 1.0 fusion.20
  175.4 24.6 %all-gather.14.cloned.1.call-done = bf16[512,2048]{1,0:T(8,128)(2,1)} async-done(((bf16[128,2048]{1,0:T(8,128)(2,1)}), bf16[512,2048]{1,0:T(8,128)(2,1)}) %all-gather.14.cloned.1.call-update) | async-done | bytes 2097168 | tf_op jit(solution)/shard_map/all_gather | solution.py:172
  200.0 126.5 %all-gather.16.cloned.1.call-done = bf16[2048,2048]{1,0:T(8,128)(2,1)} async-done(((bf16[256,2048]{1,0:T(8,128)(2,1)}), bf16[2048,2048]{1,0:T(8,128)(2,1)}) %all-gather.16.cloned.1.call-update) | async-done | bytes 8388624 | tf_op jit(solution)/shard_map/all_gather | solution.py:176
  326.4 125.0 %all-gather.18.cloned.1.call-done = bf16[2048,2048]{1,0:T(8,128)(2,1)} async-done(((bf16[2048,256]{1,0:T(8,128)(2,1)}), bf16[2048,2048]{1,0:T(8,128)(2,1)}) %all-gather.18.cloned.1.call-update) | async-done | bytes 8388624 | tf_op jit(solution)/shard_map/all_gather | solution.py:183
  451.5 16.5 %convolution_convert_fusion = bf16[512,2048]{1,0:T(8,128)(2,1)} fusion(bf16[2048,2048]{1,0:T(8,128)(2,1)} %all-gather.18.cloned.1.call-done, bf16[512,2048]{1,0:T(8,128)(2,1)} %all-gather.14.cloned.1.call-done, bf16[2048,2048]{1,0:T(8,128)(2,1)} %all-gather.16.cloned.1.call-done), kind=kOutput, calls=%fused_computation.19 | convolution fusion | flops 8594128896 | bytes 20971520 | tf_op jit(solution)/shard_map/dot_general | solution.py:181
  468.0 29.5 %reduce-scatter.2.cloned.1.call-done = bf16[128,2048]{1,0:T(8,128)(2,1)} async-done(((bf16[512,2048]{1,0:T(8,128)(2,1)}), bf16[128,2048]{1,0:T(8,128)(2,1)}) %reduce-scatter.2.cloned.1.call-update) | async-done | bytes 524304 | tf_op jit(solution)/shard_map/reduce_scatter | solution.py:186
  497.5 1.2 fusion.16
  498.8 2.1 fusion.21
  (121 shorter events, 9.3 us)
Async XLA Ops:
  6.5 2.8 copy-start.7
  6.5 159.7 %all-gather.10.cloned.1.call-start = ((), (), s32[]{:S(2)}) async-start(), calls=%async_computation.3 | async-start | bytes 7864320 | tf_op jit(solution)/shard_map/all_gather | solution.py:164
  7.3 163.3 %all-gather.12.cloned.1.call-start = ((), (), s32[]{:S(2)}) async-start(), calls=%async_computation.4 | async-start | bytes 2621440 | tf_op jit(solution)/shard_map/all_gather | solution.py:165
  9.6 2.5 copy-start.17
  10.2 3.2 copy-start.6
  14.4 45.7 %copy-start.18 = (f32[2,512]{1,0:T(2,128)S(1)}, f32[2,512]{1,0:T(2,128)}, u32[]{:S(2)}) copy-start(f32[2,512]{1,0:T(2,128)} %param.33) | copy-start | bytes 12292
  62.2 74.0 %copy-start = (f32[4,128,2]{2,1,0:T(8,128)}, f32[4,128,2]{2,1,0:T(8,128)S(1)}, u32[]{:S(2)}) copy-start(f32[4,128,2]{2,1,0:T(8,128)S(1)} %reduce_window_sum.45) | copy-start | bytes 12292
  62.9 1.0 copy-start.12
  144.7 11.0 %copy-start.1 = (f32[4,128,2]{2,1,0:T(8,128)S(1)}, f32[4,128,2]{2,1,0:T(8,128)}, u32[]{:S(2)}) copy-start(f32[4,128,2]{2,1,0:T(8,128)} %copy-done) | copy-start | bytes 12292
  144.7 11.1 %copy-start.8 = (bf16[2,4,4,8,128]{4,3,2,1,0:T(8,128)(2,1)S(1)}, bf16[2,4,4,8,128]{4,3,2,1,0:T(8,128)(2,1)}, u32[]{:S(2)}) copy-start(bf16[2,4,4,8,128]{4,3,2,1,0:T(8,128)(2,1)} %get-tuple-element.233) | copy-start | bytes 196612
  147.8 7.5 %copy-start.13 = (f32[4,1,2]{0,2,1:T(2,128)S(1)}, f32[4,1,2]{0,2,1:T(2,128)}, u32[]{:S(2)}) copy-start(f32[4,1,2]{0,2,1:T(2,128)} %copy-done.12) | copy-start | bytes 100
  147.8 7.7 %copy-start.2 = (f32[4,128,2]{2,1,0:T(8,128)S(1)}, f32[4,128,2]{2,1,0:T(8,128)}, u32[]{:S(2)}) copy-start(f32[4,128,2]{2,1,0:T(8,128)} %get-tuple-element.236) | copy-start | bytes 12292
  147.8 8.1 %copy-start.9 = (f32[4,2,64,64]{3,2,1,0:T(8,128)S(1)}, f32[4,2,64,64]{3,2,1,0:T(8,128)}, u32[]{:S(2)}) copy-start(f32[4,2,64,64]{3,2,1,0:T(8,128)} %get-tuple-element.136) | copy-start | bytes 393220
  147.8 8.4 %copy-start.3 = (f32[4,128,2,64]{1,3,2,0:T(8,128)S(1)}, f32[4,128,2,64]{1,3,2,0:T(8,128)}, u32[]{:S(2)}) copy-start(f32[4,128,2,64]{1,3,2,0:T(8,128)} %bitcast_dynamic-update-slice_fusion.2) | copy-start | bytes 786436
  147.8 8.4 %copy-start.4 = (bf16[4,128,2,64]{1,3,2,0:T(8,128)(2,1)S(1)}, bf16[4,128,2,64]{1,3,2,0:T(8,128)(2,1)}, u32[]{:S(2)}) copy-start(bf16[4,128,2,64]{1,3,2,0:T(8,128)(2,1)} %copy.99) | copy-start | bytes 393220
  147.8 8.4 %copy-start.11 = (pred[128,128]{1,0:T(8,128)(4,1)S(1)}, pred[128,128]{1,0:T(8,128)(4,1)}, u32[]{:S(2)}) copy-start(pred[128,128]{1,0:T(8,128)(4,1)} %iota_compare_fusion) | copy-start | bytes 49156
  147.8 9.1 %copy-start.10 = (bf16[512,128]{1,0:T(8,128)(2,1)S(1)}, bf16[512,128]{1,0:T(8,128)(2,1)}, u32[]{:S(2)}) copy-start(bf16[512,128]{1,0:T(8,128)(2,1)} %param.31) | copy-start | bytes 393220
  151.8 10.8 %all-to-all-start = ((bf16[4,128,384]{1,2,0:T(8,128)(2,1)}), bf16[4,128,384]{1,2,0:T(8,128)(2,1)S(1)}, u32[]{:S(2)}, u32[]{:S(2)}) async-start(bf16[4,128,384]{1,2,0:T(8,128)(2,1)} %copy_bitcast_fusion), calls=%async_computation | async-start | bytes 786432 | tf_op jit(solution)/shard_map/all_to_all | solution.py:160
  162.7 7.9 %all-to-all-start.1 = ((bf16[4,128,128]{1,2,0:T(8,128)(2,1)}), bf16[4,128,128]{1,2,0:T(8,128)(2,1)S(1)}, u32[]{:S(2)}, u32[]{:S(2)}) async-start(bf16[4,128,128]{1,2,0:T(8,128)(2,1)} %copy_bitcast_fusion.1), calls=%async_computation.1 | async-start | bytes 262144 | tf_op jit(solution)/shard_map/all_to_all | solution.py:161
  166.0 34.0 %all-gather.14.cloned.1.call-start = ((), (), s32[]{:S(2)}) async-start(), calls=%async_computation.5 | async-start | bytes 2621440 | tf_op jit(solution)/shard_map/all_gather | solution.py:172
  170.1 2.7 copy-start.5
  170.1 2.7 copy-start.14
  170.1 3.0 copy-start.15
  174.1 152.3 %all-gather.16.cloned.1.call-start = ((), (), s32[]{:S(2)}) async-start(), calls=%async_computation.6 | async-start | bytes 9437184 | tf_op jit(solution)/shard_map/all_gather | solution.py:176
  174.7 276.8 %all-gather.18.cloned.1.call-start = ((), (), s32[]{:S(2)}) async-start(), calls=%async_computation.7 | async-start | bytes 9437184 | tf_op jit(solution)/shard_map/all_gather | solution.py:183
  175.3 323.5 %copy-start.16 = (f32[2048]{0:T(1024)S(1)}, f32[2048]{0:T(1024)}, u32[]{:S(2)}) copy-start(f32[2048]{0:T(1024)} %param.41) | copy-start | bytes 24580
  175.3 322.2 %reduce-scatter.2.cloned.1.call-start = ((), (), s32[]{:S(2)}) async-start(), calls=%async_computation.8 | async-start | bytes 2621440 | tf_op jit(solution)/shard_map/reduce_scatter | solution.py:186
Sparse Core Ops, SparseCore 0:
  8.9 49.0 all-gather.9
  59.6 22.5 all-gather.11
  174.3 25.6 all-gather.13
  201.9 124.4 all-gather.15
  328.3 123.1 all-gather.17
  468.1 29.3 reduce-scatter.1
where the time goes:
time: 509 us; the launch traced here: 508 us
  waiting for transfers between devices  313 us (61%)
  blocking collectives  88 us (17%)
  matrix products  31.6 us (6%)
  local copies, waits for them, and re-layouts  26.2 us (5%)
  other arithmetic  26.1 us (5%)
  between operations  15.2 us (3%)
  starting transfers between devices  7.16 us (1%)
    all_gather x1, waiting for transfers between devices, local(): lax.all_gather(up_weight, 'sp', axis=0, tiled=True)  126 us
    all_gather x1, waiting for transfers between devices, local(): lax.all_gather(down_weight, 'sp', axis=1, tiled=True)  125 us
    all_gather x2, blocking collectives, prefix_2(): lax.all_gather(a.astype(kind), axis)  66.6 us
    reduce_scatter x1, waiting for transfers between devices, local(): lax.psum_scatter(partial_terms.astype(jnp.bfloat16), 'tp', scatter_dimens...  29.5 us
    all_gather x1, waiting for transfers between devices, local(): block_rows = lax.all_gather(normed, 'tp', axis=0, tiled=True)  24.6 us
    unnamed x1, blocking collectives  21.4 us
    dot_general x1, matrix products, local(): jnp.dot(hidden, lax.all_gather(down_weight, 'sp', axis=1, tiled=True), pr...  16.5 us
  transfers between devices with their start and end apart: 8, of which 6 were waited for; matrix products, arithmetic and copies ran while one was open for 12% of the time, Pallas kernels for 0%

commit v1 on v0

--- a/solution.py
+++ b/solution.py
@@ -7,6 +7,13 @@
 NARROW_DIM = 64
 SPAN = 128
 epsilon = 1e-06
+
+
+def _enter_marks(page, out_dim):
+    now = lax.psum(1, "sp")
+    local_part = jnp.stack([page] * now)
+    arr_now = lax.all_to_all(local_part, "sp", 0, 0)
+    return jnp.concatenate(arr_now, axis=out_dim)
 
 
 def prefix_2(array, axis, join, neutral):
@@ -179,9 +186,7 @@
     )
     hidden = (rectified * rectified).astype(jnp.bfloat16)
     partial_terms = jnp.dot(
-        hidden,
-        lax.all_gather(down_weight, "sp", axis=1, tiled=True),
-        preferred_element_type=jnp.float32,
+        hidden, _enter_marks(down_weight, 1), preferred_element_type=jnp.float32
     )
     lowered = lax.psum_scatter(
         partial_terms.astype(jnp.bfloat16), "tp", scatter_dimension=0, tiled=True

time: 509 us -> 515 us (1.012)
  starting transfers between devices: 7.16 us -> 15.9 us
  other arithmetic: 26.1 us -> 18 us
  waiting for transfers between devices: 313 us -> 321 us
    all_to_all x0 -> x1, waiting for transfers between devices: none -> 271 us  [_enter_marks(): arr_now = lax.all_to_all(local_part, 'sp', 0, 0)]
    all_gather x1, waiting for transfers between devices: 126 us -> 0.01 us  [local(): lax.all_gather(up_weight, 'sp', axis=0, tiled=True)]
    all_gather x1 -> x0, waiting for transfers between devices: 125 us -> none  [local(): lax.all_gather(down_weight, 'sp', axis=1, tiled=True)]
    all_gather x1, waiting for transfers between devices: 24.6 us -> 12.5 us  [local(): block_rows = lax.all_gather(normed, 'tp', axis=0, tiled=True)]
    all_to_all x0 -> x1, starting transfers between devices: none -> 8.76 us  [_enter_marks(): arr_now = lax.all_to_all(local_part, 'sp', 0, 0)]
  transfers between devices with their start and end apart: 8 -> 8, of which waited for: 6 -> 5; matrix products, arithmetic and copies ran while one was open for 12% -> 10% of each run, Pallas kernels for 0% -> 0%
where the time goes in v1:
time: 515 us; the launch traced here: 514 us
  waiting for transfers between devices  321 us (62%)
  blocking collectives  87.9 us (17%)
  matrix products  31 us (6%)
  local copies, waits for them, and re-layouts  24.6 us (5%)
  other arithmetic  18 us (3%)
  starting transfers between devices  15.9 us (3%)
  between operations  15.1 us (3%)
    all_to_all x1, waiting for transfers between devices, _enter_marks(): arr_now = lax.all_to_all(local_part, 'sp', 0, 0)  271 us
    all_gather x2, blocking collectives, prefix_2(): lax.all_gather(a.astype(kind), axis)  66.8 us
    reduce_scatter x1, waiting for transfers between devices, local(): lax.psum_scatter(partial_terms.astype(jnp.bfloat16), 'tp', scatter_dimens...  30.3 us
    unnamed x1, blocking collectives  21.1 us
    dot_general x1, matrix products, local(): jnp.dot(hidden, _enter_marks(down_weight, 1), preferred_element_type=jnp....  16.5 us
    all_gather x1, waiting for transfers between devices, local(): block_rows = lax.all_gather(normed, 'tp', axis=0, tiled=True)  12.5 us
  transfers between devices with their start and end apart: 8, of which 5 were waited for; matrix products, arithmetic and copies ran while one was open for 10% of the time, Pallas kernels for 0%

profile of v1, /device:TPU:0, one launch (start us, length us, event | category | flops | bytes accessed | tf_op | source)
XLA Modules:
  0.0 514.1 jit_solution(6921613934496432781)
XLA Ops:
  6.5 0.7 all-gather.9.cloned.1.call-update
  7.3 0.7 all-gather.11.cloned.1.call-update
  8.1 1.2 copy.78
  9.7 0.5 multiply_cosine_fusion
  10.2 1.0 subtract_convert_fusion
  12.5 0.6 slice_reduce_fusion.1
  13.1 0.8 fusion.76
  14.1 0.8 fusion.33
  14.9 3.2 while.42
  15.0 0.7 bitcast_dynamic-update-slice_fusion.8
  15.8 0.7 bitcast_dynamic-update-slice_fusion.8
  16.6 0.7 bitcast_dynamic-update-slice_fusion.8
  17.4 0.7 bitcast_dynamic-update-slice_fusion.8
  18.2 36.0 %all-gather.1 = bf16[24,128,128]{2,1,0:T(8,128)(2,1)} all-gather(bf16[3,128,128]{2,1,0:T(8,128)(2,1)S(1)} %convert_element_type.154), channel_id=3, replica_groups=mesh['sp'=8,'tp'=4] {'sp'}, dimensions={0}, use_global_device_ids=true | all-gather | bytes 884736 | tf_op jit(solution)/shard_map/all_gather | solution.py:22
  54.2 0.3 multiply_cosine_fusion.1
  54.5 1.0 copy.94
  55.6 1.0 copy.107
  56.6 0.8 fusion.61
  57.4 0.7 bitcast_dynamic-update-slice_fusion.3
  58.6 0.6 copy-done.16
  59.3 0.8 fusion.74
  60.5 1.6 bitcast_dynamic-update-slice_fusion.2
  62.1 1.1 fusion.54
  63.2 2.9 while.43
  63.2 0.6 bitcast_dynamic-update-slice_fusion.9
  63.9 0.6 bitcast_dynamic-update-slice_fusion.9
  64.7 0.6 bitcast_dynamic-update-slice_fusion.9
  65.4 0.6 bitcast_dynamic-update-slice_fusion.9
  66.1 30.8 %all-gather.3 = bf16[16,64,64]{2,1,0:T(8,128)(2,1)S(1)} all-gather(bf16[2,64,64]{2,1,0:T(8,128)(2,1)S(1)} %convert_element_type.158), channel_id=5, replica_groups=mesh['sp'=8,'tp'=4] {'sp'}, dimensions={0}, use_global_device_ids=true | all-gather | bytes 147456 | tf_op jit(solution)/shard_map/all_gather | solution.py:22
  97.0 0.6 dynamic-slice
  99.4 21.1 %all-reduce.2 = (bf16[24]{0:T(256)(128)(2,1)S(1)}, bf16[16]{0:T(256)(128)(2,1)S(1)}) all-reduce(bf16[24]{0:T(256)(128)(2,1)S(1)} %dynamic-update-slice, bf16[16]{0:T(256)(128)(2,1)S(1)} %dynamic-update-slice.1), channel_id=2, replica_groups=mesh['sp'=8,'tp'=4] {'sp'}, use_global_device_ids=true, to_apply=%add | all-reduce | flops 40 | bytes 160
  120.7 0.7 concatenate.34
  121.5 1.2 copy.79
  122.6 0.7 concatenate.35
  123.4 1.2 copy.80
  124.5 0.6 subtract_exponential_fusion
  125.1 1.1 copy.103
  126.3 0.6 iota_compare_fusion
  126.9 2.7 fusion.8
  129.6 3.1 multiply_reduce_fusion.1
  132.8 1.7 copy.104
  134.5 1.2 copy.105
  136.0 0.8 copy_bitcast_fusion
  136.8 3.5 all-to-all-start
  140.9 0.3 fusion.15
  141.2 0.5 multiply_reduce_fusion.2
  142.1 0.7 copy_bitcast_fusion.1
  142.8 4.9 all-to-all-done
  147.7 3.3 all-to-all-start.1
  151.2 3.8 fusion.77
  155.1 0.5 all-to-all-done.1
  155.6 2.1 multiply_reduce_fusion
  157.7 0.4 fusion.18
  158.1 1.0 fusion.20
  159.1 0.6 copy.119
  159.8 4.3 stack.2
  164.1 8.8 %all-to-all-start.2 = ((bf16[8,2048,256]{1,2,0:T(8,128)(2,1)}), bf16[8,2048,256]{1,2,0:T(8,128)(2,1)}, u32[]{:S(2)}, u32[]{:S(2)}) async-start(bf16[8,2048,256]{1,2,0:T(8,128)(2,1)} %stack.2), calls=%async_computation.2 | async-start | bytes 16777216 | tf_op jit(solution)/shard_map/all_to_all | solution.py:15
  172.9 0.5 all-gather.15.cloned.1.call-update
  173.5 12.5 %all-gather.13.cloned.1.call-done = bf16[512,2048]{1,0:T(8,128)(2,1)} async-done(((bf16[128,2048]{1,0:T(8,128)(2,1)}), bf16[512,2048]{1,0:T(8,128)(2,1)}) %all-gather.13.cloned.1.call-update) | async-done | bytes 2097168 | tf_op jit(solution)/shard_map/all_gather | solution.py:179
  185.9 271.4 %all-to-all-done.2 = bf16[8,2048,256]{1,2,0:T(8,128)(2,1)} async-done(((bf16[8,2048,256]{1,2,0:T(8,128)(2,1)}), bf16[8,2048,256]{1,2,0:T(8,128)(2,1)}, u32[]{:S(2)}, u32[]{:S(2)}) %all-to-all-start.2) | async-done | bytes 8388640 | tf_op jit(solution)/shard_map/all_to_all | solution.py:15
  457.4 16.5 %convolution_convert_fusion = bf16[512,2048]{1,0:T(8,128)(2,1)} fusion(bf16[2048,2048]{0,1:T(8,128)(2,1)} %bitcast.37, bf16[512,2048]{1,0:T(8,128)(2,1)} %all-gather.13.cloned.1.call-done, bf16[2048,2048]{1,0:T(8,128)(2,1)} %all-gather.15.cloned.1.call-done), kind=kOutput, calls=%fused_computation.19 | convolution fusion | flops 8594128896 | bytes 20971520 | tf_op jit(solution)/shard_map/dot_general | solution.py:188
  473.9 30.3 %reduce-scatter.2.cloned.1.call-done = bf16[128,2048]{1,0:T(8,128)(2,1)} async-done(((bf16[512,2048]{1,0:T(8,128)(2,1)}), bf16[128,2048]{1,0:T(8,128)(2,1)}) %reduce-scatter.2.cloned.1.call-update) | async-done | bytes 524304 | tf_op jit(solution)/shard_map/reduce_scatter | solution.py:191
  504.2 1.2 fusion.16
  505.5 2.1 fusion.21
  (134 shorter events, 6.3 us)
Async XLA Ops:
  6.5 2.8 copy-start.9
  6.5 144.7 %all-gather.9.cloned.1.call-start = ((), (), s32[]{:S(2)}) async-start(), calls=%async_computation.4 | async-start | bytes 7864320 | tf_op jit(solution)/shard_map/all_gather | solution.py:171
  7.3 148.3 %all-gather.11.cloned.1.call-start = ((), (), s32[]{:S(2)}) async-start(), calls=%async_computation.5 | async-start | bytes 2621440 | tf_op jit(solution)/shard_map/all_gather | solution.py:172
  9.6 2.5 copy-start.21
  10.2 3.8 copy-start.8
  14.9 43.2 %copy-start.22 = (f32[2,512]{1,0:T(2,128)S(1)}, f32[2,512]{1,0:T(2,128)}, u32[]{:S(2)}) copy-start(f32[2,512]{1,0:T(2,128)} %param.33) | copy-start | bytes 12292
  14.9 45.2 %copy-start.13 = (bf16[512,128]{1,0:T(8,128)(2,1)S(1)}, bf16[512,128]{1,0:T(8,128)(2,1)}, u32[]{:S(2)}) copy-start(bf16[512,128]{1,0:T(8,128)(2,1)} %param.30) | copy-start | bytes 393220
  54.5 42.4 %copy-start.23 = (f32[3]{0:T(128)S(1)}, f32[3]{0:T(128)}, u32[]{:S(2)}) copy-start(f32[3]{0:T(128)} %get-tuple-element.242) | copy-start | bytes 40
  54.5 42.5 %copy-start.24 = (u32[32]{0:T(128)S(1)}, u32[32]{0:T(128)}, u32[]{:S(2)}) copy-start(u32[32]{0:T(128)} %constant.117) | copy-start | bytes 388
  58.5 62.2 %copy-start = (f32[4,128,2]{2,1,0:T(8,128)}, f32[4,128,2]{2,1,0:T(8,128)S(1)}, u32[]{:S(2)}) copy-start(f32[4,128,2]{2,1,0:T(8,128)S(1)} %reduce_window_sum.45) | copy-start | bytes 12292
  58.6 0.6 copy-start.16
  60.1 60.7 %copy-start.5 = (bf16[512,3,64]{0,2,1:T(8,128)(2,1)S(1)}, bf16[512,3,64]{0,2,1:T(8,128)(2,1)}, u32[]{:S(2)}) copy-start(bf16[512,3,64]{0,2,1:T(8,128)(2,1)} %get-tuple-element.228) | copy-start | bytes 589828
  60.3 62.3 %copy-start.4 = (bf16[512,3,64]{0,2,1:T(8,128)(2,1)S(1)}, bf16[512,3,64]{0,2,1:T(8,128)(2,1)}, u32[]{:S(2)}) copy-start(bf16[512,3,64]{0,2,1:T(8,128)(2,1)} %get-tuple-element.229) | copy-start | bytes 589828
  129.6 11.1 %copy-start.1 = (f32[4,128,2]{2,1,0:T(8,128)S(1)}, f32[4,128,2]{2,1,0:T(8,128)}, u32[]{:S(2)}) copy-start(f32[4,128,2]{2,1,0:T(8,128)} %copy-done) | copy-start | bytes 12292
  132.8 7.5 %copy-start.17 = (f32[4,1,2]{0,2,1:T(2,128)S(1)}, f32[4,1,2]{0,2,1:T(2,128)}, u32[]{:S(2)}) copy-start(f32[4,1,2]{0,2,1:T(2,128)} %copy-done.16) | copy-start | bytes 100
  132.8 7.7 %copy-start.2 = (f32[4,128,2]{2,1,0:T(8,128)S(1)}, f32[4,128,2]{2,1,0:T(8,128)}, u32[]{:S(2)}) copy-start(f32[4,128,2]{2,1,0:T(8,128)} %get-tuple-element.236) | copy-start | bytes 12292
  132.8 8.1 %copy-start.11 = (bf16[2,4,4,8,128]{4,3,2,1,0:T(8,128)(2,1)S(1)}, bf16[2,4,4,8,128]{4,3,2,1,0:T(8,128)(2,1)}, u32[]{:S(2)}) copy-start(bf16[2,4,4,8,128]{4,3,2,1,0:T(8,128)(2,1)} %get-tuple-element.233) | copy-start | bytes 196612
  132.8 8.1 %copy-start.10 = (bf16[2,4,4,8,128]{4,3,2,1,0:T(8,128)(2,1)S(1)}, bf16[2,4,4,8,128]{4,3,2,1,0:T(8,128)(2,1)}, u32[]{:S(2)}) copy-start(bf16[2,4,4,8,128]{4,3,2,1,0:T(8,128)(2,1)} %get-tuple-element.232) | copy-start | bytes 196612
  132.8 8.1 %copy-start.12 = (f32[4,2,64,64]{3,2,1,0:T(8,128)S(1)}, f32[4,2,64,64]{3,2,1,0:T(8,128)}, u32[]{:S(2)}) copy-start(f32[4,2,64,64]{3,2,1,0:T(8,128)} %get-tuple-element.136) | copy-start | bytes 393220
  132.8 8.4 %copy-start.6 = (f32[4,128,2,64]{1,3,2,0:T(8,128)S(1)}, f32[4,128,2,64]{1,3,2,0:T(8,128)}, u32[]{:S(2)}) copy-start(f32[4,128,2,64]{1,3,2,0:T(8,128)} %bitcast_dynamic-update-slice_fusion.2) | copy-start | bytes 786436
  132.8 8.4 %copy-start.15 = (pred[128,128]{1,0:T(8,128)(4,1)S(1)}, pred[128,128]{1,0:T(8,128)(4,1)}, u32[]{:S(2)}) copy-start(pred[128,128]{1,0:T(8,128)(4,1)} %iota_compare_fusion) | copy-start | bytes 49156
  132.8 9.1 %copy-start.14 = (bf16[512,128]{1,0:T(8,128)(2,1)S(1)}, bf16[512,128]{1,0:T(8,128)(2,1)}, u32[]{:S(2)}) copy-start(bf16[512,128]{1,0:T(8,128)(2,1)} %param.31) | copy-start | bytes 393220
  136.8 10.8 %all-to-all-start = ((bf16[4,128,384]{1,2,0:T(8,128)(2,1)}), bf16[4,128,384]{1,2,0:T(8,128)(2,1)S(1)}, u32[]{:S(2)}, u32[]{:S(2)}) async-start(bf16[4,128,384]{1,2,0:T(8,128)(2,1)} %copy_bitcast_fusion), calls=%async_computation | async-start | bytes 786432 | tf_op jit(solution)/shard_map/all_to_all | solution.py:167
  147.7 7.9 %all-to-all-start.1 = ((bf16[4,128,128]{1,2,0:T(8,128)(2,1)}), bf16[4,128,128]{1,2,0:T(8,128)(2,1)S(1)}, u32[]{:S(2)}, u32[]{:S(2)}) async-start(bf16[4,128,128]{1,2,0:T(8,128)(2,1)} %copy_bitcast_fusion.1), calls=%async_computation.1 | async-start | bytes 262144 | tf_op jit(solution)/shard_map/all_to_all | solution.py:168
  151.0 35.0 %all-gather.13.cloned.1.call-start = ((), (), s32[]{:S(2)}) async-start(), calls=%async_computation.6 | async-start | bytes 2621440 | tf_op jit(solution)/shard_map/all_gather | solution.py:179
  155.0 2.7 copy-start.7
  155.1 2.7 copy-start.18
  155.1 3.0 copy-start.19
  155.1 4.0 copy-start.3
  164.1 293.2 %all-to-all-start.2 = ((bf16[8,2048,256]{1,2,0:T(8,128)(2,1)}), bf16[8,2048,256]{1,2,0:T(8,128)(2,1)}, u32[]{:S(2)}, u32[]{:S(2)}) async-start(bf16[8,2048,256]{1,2,0:T(8,128)(2,1)} %stack.2), calls=%async_computation.2 | async-start | bytes 16777216 | tf_op jit(solution)/shard_map/all_to_all | solution.py:15
  172.9 284.5 %all-gather.15.cloned.1.call-start = ((), (), s32[]{:S(2)}) async-start(), calls=%async_computation.7 | async-start | bytes 9437184 | tf_op jit(solution)/shard_map/all_gather | solution.py:183
  173.4 330.8 %reduce-scatter.2.cloned.1.call-start = ((), (), s32[]{:S(2)}) async-start(), calls=%async_computation.8 | async-start | bytes 2621440 | tf_op jit(solution)/shard_map/reduce_scatter | solution.py:191
  457.3 48.1 %copy-start.20 = (f32[2048]{0:T(1024)S(1)}, f32[2048]{0:T(1024)}, u32[]{:S(2)}) copy-start(f32[2048]{0:T(1024)} %param.41) | copy-start | bytes 24580
Sparse Core Ops, SparseCore 0:
  8.9 49.1 all-gather.8
  59.6 22.5 all-gather.10
  159.2 26.6 all-gather.12
  187.9 259.5 all-gather.14
  474.0 30.1 reduce-scatter.1
